TPU v7x, 32 devices: a whole 2x2x4 slice. The times are simulated.
32 devices in a mesh: sp: 16 (over z, y, x), tp: 2 (over core).
Axes of the slice: x: 2, y: 2, z: 4, core: 2. Of those that a mesh axis runs over, the one named last changes fastest.
Arguments:
- tokens: bfloat16 [4096, 2048], P(('sp', 'tp')), may hold values from -6 to 6
- gain: float32 [2048], replicated, may hold values from 0.1 to 1.9
- w_ret_q: bfloat16 [2048, 2048], P(None, 'tp'), may hold values from -0.125 to 0.125
- w_ret_k: bfloat16 [2048, 2048], P(None, 'tp'), may hold values from -0.125 to 0.125
- w_ret_v: bfloat16 [2048, 2048], P(None, 'tp'), may hold values from -0.125 to 0.125
- w_fox_q: bfloat16 [2048, 1024], P(None, 'tp'), may hold values from -0.125 to 0.125
- w_fox_k: bfloat16 [2048, 1024], P(None, 'tp'), may hold values from -0.125 to 0.125
- w_fox_v: bfloat16 [2048, 1024], P(None, 'tp'), may hold values from -0.125 to 0.125
- fox_gates: float32 [4096, 8], P('sp', 'tp'), may hold values from -4096 to 0, as said below
- w_out_ret: bfloat16 [2048, 2048], P('tp', 'sp'), may hold values from -0.109375 to 0.109375
- w_out_fox: bfloat16 [1024, 2048], P('tp', 'sp'), may hold values from -0.109375 to 0.109375
Outputs:
- mixed: bfloat16 [4096, 2048], P(('sp', 'tp'))
Inputs may be any that keep to these rules, and one draw needn't show every extreme that they name: `fox_gates`: each head's values never rise along positions.
All inputs are finite; a program needn't handle non-finite values.
Results may differ from a plain program's by a relative error of at most 0.02.
Values may be sent and summed in bfloat16 or wider, within the bound.
A program may use at most 128 MiB of HBM per device.

v0:
```python
import math
import jax
import jax.numpy as jnp
from jax import lax
from jax.sharding import PartitionSpec as P

RET_HEADS = 8
RET_DIM = 256
FOX_DIM = 128
BLOCK = 128
eps = 1e-06


def prefix(part, axis, combine, identity):
    place = lax.axis_index(axis)
    gathered = jax.tree.map(lambda a: lax.all_gather(a, axis), part)
    state = jax.tree.map(lambda a, e: jnp.zeros_like(a) + jnp.asarray(e, a.dtype), part, identity)

    def one(lap, state):
        return combine(
            state, jax.tree.map(lambda a: lax.dynamic_index_in_dim(a, lap, 0, False), gathered)
        )

    return lax.fori_loop(0, place, one, state)


def head_norm(values, width):
    rows_here = values.shape[0]
    grouped = values.reshape(rows_here, -1, width)
    scaled = grouped * lax.rsqrt(jnp.mean(grouped * grouped, axis=2, keepdims=True) + eps)
    return scaled.reshape(rows_here, -1).astype(jnp.bfloat16)


def rotate(values, token_positions, width):
    rows_here = values.shape[0]
    half_width = width // 2
    inverse = 10000.0 ** (-jnp.arange(half_width, dtype=jnp.float32) / half_width)
    angles = token_positions.astype(jnp.float32)[:, None] * inverse[None, :]
    cosine = jnp.cos(angles)[:, None, :]
    sine = jnp.sin(angles)[:, None, :]
    grouped = values.astype(jnp.float32).reshape(rows_here, -1, width)
    first_half = grouped[..., :half_width]
    second_half = grouped[..., half_width:]
    turned = jnp.concatenate(
        [first_half * cosine - second_half * sine, first_half * sine + second_half * cosine],
        axis=-1,
    )
    return turned.reshape(rows_here, -1)


def decay_rates(head_ids, total):
    heads_float = head_ids.astype(jnp.float32)
    middle = RET_HEADS // 2
    fast_rate = 1.0 / (32.0 + 16.0 * heads_float)
    slow_rate = jnp.exp2(-(heads_float - middle)) / total
    return jnp.where(head_ids < middle, fast_rate, slow_rate)


def decay_tables(rates):
    offsets = jnp.arange(BLOCK, dtype=jnp.float32)
    spread = offsets[:, None] - offsets[None, :]
    causal = spread >= 0
    within = jnp.where(
        causal[None], jnp.exp(-rates[:, None, None] * jnp.where(causal, spread, 0.0)[None]), 0.0
    )
    query_decay = jnp.exp(-rates[None, :] * (offsets[:, None] + 1.0))
    key_decay = jnp.exp(-rates[None, :] * (BLOCK - 1.0 - offsets[:, None]))
    block_decay = jnp.exp(-rates * BLOCK)
    return (within, query_decay, key_decay, block_decay)


def advance(carry, key_block, value_block, key_decay, block_decay):
    scaled = (key_block.astype(jnp.float32) * key_decay[:, :, None]).astype(jnp.bfloat16)
    update = jnp.einsum("shd,she->hde", scaled, value_block, preferred_element_type=jnp.float32)
    return carry * block_decay[:, None, None] + update


def retention_blocks(queries, keys, values, rates, state, heads):
    within, query_decay, key_decay, block_decay = decay_tables(rates)
    count = queries.shape[0] // BLOCK

    def shaped(array):
        return array.reshape(count, BLOCK, heads, RET_DIM)

    def retention_step(carry, blocks):
        query_block, key_block, value_block = blocks
        scores = (
            jnp.einsum("thd,shd->hts", query_block, key_block, preferred_element_type=jnp.float32)
            * within
        )
        inner = jnp.einsum(
            "hts,she->the",
            scores.astype(jnp.bfloat16),
            value_block,
            preferred_element_type=jnp.float32,
        )
        cross = (
            jnp.einsum(
                "thd,hde->the",
                query_block.astype(jnp.float32),
                carry,
                precision=lax.Precision.HIGHEST,
            )
            * query_decay[:, :, None]
        )
        return (advance(carry, key_block, value_block, key_decay, block_decay), inner + cross)

    final_state, outputs = lax.scan(
        retention_step, state, (shaped(queries), shaped(keys), shaped(values))
    )
    return (final_state, outputs.reshape(count * BLOCK, heads * RET_DIM))


def block_states(keys, values, rates, heads):
    _, _, key_decay, block_decay = decay_tables(rates)
    count = keys.shape[0] // BLOCK

    def block_step(carry, blocks):
        return (advance(carry, blocks[0], blocks[1], key_decay, block_decay), None)

    start_state = jnp.zeros((heads, RET_DIM, RET_DIM), jnp.float32)
    blocks = (
        keys.reshape(count, BLOCK, heads, RET_DIM),
        values.reshape(count, BLOCK, heads, RET_DIM),
    )
    final_state, _ = lax.scan(block_step, start_state, blocks)
    return final_state


def join_states(earlier, later):
    return (earlier[0] * later[0], earlier[1] * later[0][:, None, None] + later[1])


def fox_weights(queries, keys, query_gates, key_gates, query_pos, key_pos):
    scores = jnp.einsum(
        "qhd,khd->hqk", queries, keys, preferred_element_type=jnp.float32
    ) * FOX_DIM ** (-0.5)
    scores = scores + query_gates.T[:, :, None] - key_gates.T[:, None, :]
    allowed = key_pos[None, :] <= query_pos[:, None]
    return jnp.exp(jnp.where(allowed[None], scores, -jnp.inf))


def add_block(numer, denom, weights, values):
    numer = numer + jnp.einsum(
        "hqk,khd->qhd", weights.astype(jnp.bfloat16), values, preferred_element_type=jnp.float32
    )
    denom = denom + jnp.sum(weights, axis=2).T
    return (numer, denom)


def per_device(
    tokens,
    gain,
    w_ret_q,
    w_ret_k,
    w_ret_v,
    w_fox_q,
    w_fox_k,
    w_fox_v,
    fox_gates,
    w_out_ret,
    w_out_fox,
):
    inputs = tokens.astype(jnp.float32)
    normed = (
        inputs * lax.rsqrt(jnp.mean(inputs * inputs, axis=1, keepdims=True) + eps) * gain
    ).astype(jnp.bfloat16)
    weights_in = (w_ret_q, w_ret_k, w_ret_v, w_fox_q, w_fox_k, w_fox_v)
    piece = lax.all_gather(normed, "tp", axis=0, tiled=True)
    products = [jnp.dot(piece, matrix, preferred_element_type=jnp.float32) for matrix in weights_in]
    projected = jnp.concatenate(products, axis=1).astype(jnp.bfloat16)
    ret_width = w_ret_q.shape[1]
    fox_width = w_fox_q.shape[1]
    edges = [
        0,
        ret_width,
        2 * ret_width,
        3 * ret_width,
        3 * ret_width + fox_width,
        3 * ret_width + 2 * fox_width,
        3 * ret_width + 3 * fox_width,
    ]
    pieces_out = [projected[:, edges[column] : edges[column + 1]] for column in range(6)]
    ret_query, ret_key, ret_value, fox_query, fox_key, fox_value = pieces_out
    length = projected.shape[0]
    sp_count = lax.axis_size("sp")
    total = length * sp_count
    offset = lax.axis_index("sp") * length
    token_positions = offset + jnp.arange(length, dtype=jnp.int32)
    ret_heads = ret_width // RET_DIM
    fox_heads = fox_width // FOX_DIM
    head_ids = lax.axis_index("tp") * ret_heads + jnp.arange(ret_heads, dtype=jnp.int32)
    rates = decay_rates(head_ids, float(total))
    query_rot = rotate(ret_query, token_positions, RET_DIM).astype(jnp.bfloat16)
    key_rot = (rotate(ret_key, token_positions, RET_DIM) * RET_DIM ** (-0.5)).astype(jnp.bfloat16)
    span_decay = jnp.exp(-rates * length)
    empty_state = jnp.zeros((ret_heads, RET_DIM, RET_DIM), jnp.float32)
    identity = (jnp.ones_like(span_decay), empty_state)
    final_state = block_states(key_rot, ret_value, rates, ret_heads)
    carried = prefix((span_decay, final_state), "sp", join_states, identity)[1]
    ret_raw = retention_blocks(query_rot, key_rot, ret_value, rates, carried, ret_heads)[1]
    ret_mixed = head_norm(ret_raw, RET_DIM)
    gates_all = lax.all_gather(fox_gates, "sp", axis=0, tiled=True)
    query3 = fox_query.reshape(length, fox_heads, FOX_DIM)
    zero_numer = jnp.zeros((length, fox_heads, FOX_DIM), jnp.float32)
    zero_denom = jnp.zeros((length, fox_heads), jnp.float32)
    last_query = offset + length - 1
    keys = lax.all_gather(fox_key, "sp", axis=0, tiled=True)
    values = lax.all_gather(fox_value, "sp", axis=0, tiled=True)
    rows_here = keys.shape[0]
    width = math.gcd(rows_here, 512)

    def one_block(state, index):
        begin = index * width

        def compute(accum):
            key_block = lax.dynamic_slice_in_dim(keys, begin, width, 0).reshape(
                width, fox_heads, FOX_DIM
            )
            value_block = lax.dynamic_slice_in_dim(values, begin, width, 0).reshape(
                width, fox_heads, FOX_DIM
            )
            key_gates = lax.dynamic_slice_in_dim(gates_all, begin, width, 0)
            key_pos = begin + jnp.arange(width, dtype=jnp.int32)
            weights = fox_weights(query3, key_block, fox_gates, key_gates, token_positions, key_pos)
            return add_block(accum[0], accum[1], weights, value_block)

        def skip(accum):
            return accum

        return (lax.cond(begin <= last_query, compute, skip, state), None)

    result, _ = lax.scan(
        one_block, (zero_numer, zero_denom), jnp.arange(rows_here // width, dtype=jnp.int32)
    )
    numer, denom = result
    fox_raw = (numer / denom[:, :, None]).reshape(length, fox_width)
    fox_mixed = head_norm(fox_raw, FOX_DIM)
    out_ret, out_fox = (
        lax.all_gather(w_out_ret, "sp", axis=1, tiled=True),
        lax.all_gather(w_out_fox, "sp", axis=1, tiled=True),
    )
    return lax.psum_scatter(
        (
            jnp.dot(ret_mixed, out_ret, preferred_element_type=jnp.float32)
            + jnp.dot(fox_mixed, out_fox, preferred_element_type=jnp.float32)
        ).astype(jnp.bfloat16),
        "tp",
        scatter_dimension=0,
        tiled=True,
    )


def solution(mesh):
    in_specs = (
        P(("sp", "tp"), None),
        P(),
        P(None, "tp"),
        P(None, "tp"),
        P(None, "tp"),
        P(None, "tp"),
        P(None, "tp"),
        P(None, "tp"),
        P("sp", "tp"),
        P("tp", "sp"),
        P("tp", "sp"),
    )
    out_specs = P(("sp", "tp"), None)
    return jax.shard_map(
        per_device, mesh=mesh, in_specs=in_specs, out_specs=out_specs, check_vma=False
    )
```

profile of v0, /device:TPU:0, one launch (start us, length us, event | category | flops | bytes accessed | tf_op | source)
XLA Modules:
  0.0 542.5 jit_solution(13365814762456692468)
XLA Ops:
  6.5 1.4 fusion.62
  7.9 2.0 fusion.64
  10.0 11.9 %all-gather.9.cloned.1.call-done = bf16[256,2048]{1,0:T(8,128)(2,1)} async-done(((bf16[128,2048]{1,0:T(8,128)(2,1)}), bf16[256,2048]{1,0:T(8,128)(2,1)}) %all-gather.9.cloned.1.call-update) | async-done | bytes 1048592 | tf_op jit(solution)/shard_map/all_gather | solution.py:169
  21.9 2.7 convolution_convert_fusion.5
  24.7 3.0 convolution_convert_fusion.4
  28.4 3.4 fusion.60
  32.3 3.9 fusion.59
  36.3 1.5 reshape.289
  37.8 3.8 convolution_convert_fusion.1
  42.0 1.4 fusion.71
  43.8 1.4 while.52
  45.2 1.0 copy-done.2
  47.6 41.5 %all-gather.1 = f32[16,1,4]{2,1,0:T(1,128)S(1)} all-gather(f32[1,1,4]{2,1,0:T(1,128)S(1)} %exponential_bitcast_fusion), channel_id=1, replica_groups=mesh['sp'=16,'tp'=2] {'sp'}, dimensions={0}, use_global_device_ids=true | all-gather | bytes 272 | tf_op jit(solution)/shard_map/all_gather | solution.py:16
  89.1 36.1 %all_gather.35 = f32[4096,4]{0,1:T(4,128)S(1)} all-gather(f32[256,4]{0,1:T(4,128)S(1)} %copy-done.4), channel_id=1, replica_groups=mesh['sp'=16,'tp'=2] {'sp'}, dimensions={0}, use_global_device_ids=true | all-gather | bytes 69632 | tf_op jit(solution)/shard_map/all_gather | solution.py:203
  125.2 2.6 fusion.61
  128.0 6.5 %copy.78 = bf16[4096,512]{0,1:T(8,128)(2,1)} copy(bf16[4096,512]{1,0:T(8,128)(2,1)} %all-gather.13.cloned.1.call-done) | data formatting | bytes 8388608
  134.5 44.9 %all-gather.15.cloned.1.call-done = bf16[4096,512]{1,0:T(8,128)(2,1)} async-done(((bf16[256,512]{1,0:T(8,128)(2,1)}), bf16[4096,512]{1,0:T(8,128)(2,1)}) %all-gather.15.cloned.1.call-update) | async-done | bytes 4194320 | tf_op jit(solution)/shard_map/all_gather | solution.py:208
  179.4 6.4 %copy.79 = bf16[4096,512]{0,1:T(8,128)(2,1)} copy(bf16[4096,512]{1,0:T(8,128)(2,1)} %all-gather.15.cloned.1.call-done) | data formatting | bytes 8388608
  185.8 13.7 %while.51 = (s32[]{:T(128)}, f32[256,4,128]{0,2,1:T(8,128)S(1)}, f32[256,4]{0,1:T(4,128)S(1)}, s32[8]{0:T(128)S(1)}, s32[]{:T(128)}, /*index=5*/bf16[4096,512]{0...) while((s32[]{:T(128)}, f32[256,4,128]{0,2,1:T(8,128)S(1)}, ...), condition=%wide.region_12.13_spmd.clone, body=%wide.region_8.12_spmd.clone.sunk | while | flops 271844096 | bytes 6869325 | solution.py:233
  187.1 3.4 conditional.3
  187.1 1.9 constant_dynamic-slice_fusion
  189.2 0.9 fusion.70
  199.7 171.9 %all-gather.19.cloned.1.call-done = f32[64,256,256]{2,1,0:T(8,128)} async-done(((f32[4,256,256]{2,1,0:T(8,128)}), f32[64,256,256]{2,1,0:T(8,128)}) %all-gather.19.cloned.1.call-update) | async-done | bytes 16777232 | tf_op jit(solution)/shard_map/all_gather | solution.py:16
  371.9 6.1 %while.53 = (s32[]{:T(128)}, f32[4,256,256]{2,1,0:T(8,128)S(1)}, f32[2,128,4,256]{1,3,2,0:T(8,128)}, bf16[2,128,4,256]{3,1,0,2:T(8,128)(2,1)S(1)}, bf16[2,128,4,...) while((s32[]{:T(128)}, f32[4,256,256]{2,1,0:T(8,128)S(1)}, ...), condition=%wide.region_6.7_spmd.clone.clone, body=%wide.region_5.6_spmd.clone.clone.sunk | while | flops 538313792 | bytes 6387361 | solution.py:108
  372.4 1.9 fusion.110
  375.5 1.9 fusion.110
  378.0 1.7 copy.76
  380.7 80.4 %all-gather.11.cloned.1.call-done = bf16[1024,2048]{1,0:T(8,128)(2,1)} async-done(((bf16[1024,128]{1,0:T(8,128)(2,1)}), bf16[1024,2048]{1,0:T(8,128)(2,1)}) %all-gather.11.cloned.1.call-update) | async-done | bytes 4194320 | tf_op jit(solution)/shard_map/all_gather | solution.py:240
  461.1 4.8 fusion.66
  465.9 58.9 %all-gather.17.cloned.1.call-done = bf16[512,2048]{1,0:T(8,128)(2,1)} async-done(((bf16[512,128]{1,0:T(8,128)(2,1)}), bf16[512,2048]{1,0:T(8,128)(2,1)}) %all-gather.17.cloned.1.call-update) | async-done | bytes 2097168 | tf_op jit(solution)/shard_map/all_gather | solution.py:241
  524.8 4.1 fusion.58
  528.9 6.7 %reduce-scatter.2.cloned.1.call-done = bf16[128,2048]{1,0:T(8,128)(2,1)} async-done(((bf16[256,2048]{1,0:T(8,128)(2,1)}), bf16[128,2048]{1,0:T(8,128)(2,1)}) %reduce-scatter.2.cloned.1.call-update) | async-done | bytes 524304 | tf_op jit(solution)/shard_map/reduce_scatter | solution.py:243
  (105 shorter events, 13.9 us)
Async XLA Ops:
  6.5 15.4 %copy-start = (bf16[2048,512]{1,0:T(8,128)(2,1)S(1)}, bf16[2048,512]{1,0:T(8,128)(2,1)}, u32[]{:S(2)}) copy-start(bf16[2048,512]{1,0:T(8,128)(2,1)} %param.28) | copy-start | bytes 6291460
  6.5 15.3 %all-gather.9.cloned.1.call-start = ((), (), s32[]{:S(2)}) async-start(), calls=%async_computation.1 | async-start | bytes 1572864 | tf_op jit(solution)/shard_map/all_gather | solution.py:169
  10.0 118.0 %all-gather.13.cloned.1.call-start = ((), (), s32[]{:S(2)}) async-start(), calls=%async_computation.3 | async-start | bytes 4456448 | tf_op jit(solution)/shard_map/all_gather | solution.py:209
  21.9 2.8 copy-start.5
  24.6 154.7 %all-gather.15.cloned.1.call-start = ((), (), s32[]{:S(2)}) async-start(), calls=%async_computation.4 | async-start | bytes 4456448 | tf_op jit(solution)/shard_map/all_gather | solution.py:208
  27.7 343.9 %all-gather.19.cloned.1.call-start = ((), (), s32[]{:S(2)}) async-start(), calls=%async_computation.7 | async-start | bytes 17825792 | tf_op jit(solution)/shard_map/all_gather | solution.py:16
  43.8 45.3 %copy-start.4 = (f32[256,4]{0,1:T(4,128)S(1)}, f32[256,4]{0,1:T(4,128)}, u32[]{:S(2)}) copy-start(f32[256,4]{0,1:T(4,128)} %param.29) | copy-start | bytes 12292
  45.2 1.0 copy-start.2
  46.3 414.9 %all-gather.11.cloned.1.call-start = ((), (), s32[]{:S(2)}) async-start(), calls=%async_computation.2 | async-start | bytes 4456448 | tf_op jit(solution)/shard_map/all_gather | solution.py:240
  46.9 478.0 %all-gather.17.cloned.1.call-start = ((), (), s32[]{:S(2)}) async-start(), calls=%async_computation.5 | async-start | bytes 2228224 | tf_op jit(solution)/shard_map/all_gather | solution.py:241
  47.4 488.2 %reduce-scatter.2.cloned.1.call-start = ((), (), s32[]{:S(2)}) async-start(), calls=%async_computation.6 | async-start | bytes 1572864 | tf_op jit(solution)/shard_map/reduce_scatter | solution.py:243
  378.0 1.7 copy-start.3
  524.8 10.8 %copy-start.1 = (bf16[2048,512]{1,0:T(8,128)(2,1)S(1)}, bf16[2048,512]{1,0:T(8,128)(2,1)}, u32[]{:S(2)}) copy-start(bf16[2048,512]{1,0:T(8,128)(2,1)} %param.28) | copy-start | bytes 6291460
Sparse Core Ops, SparseCore 0:
  10.1 11.7 all-gather.8
  24.8 77.4 all-gather.12
  105.0 74.3 all-gather.14
  182.0 189.5 all-gather.18
  374.2 86.8 all-gather.10
  463.7 61.1 all-gather.16
  529.0 6.5 reduce-scatter.1
where the time goes:
time: 544 us; the launch traced here: 543 us
  waiting for transfers between devices  376 us (69%)
  blocking collectives  77.7 us (14%)
  matrix products  36.2 us (7%)
  local copies, waits for them, and re-layouts  27.5 us (5%)
  between operations  13.8 us (3%)
  loops' own time  5.99 us (1%)
    all_gather x1, waiting for transfers between devices, prefix(): gathered = jax.tree.map(lambda a: lax.all_gather(a, axis), part)  172 us
    all_gather x1, waiting for transfers between devices, per_device(): lax.all_gather(w_out_ret, 'sp', axis=1, tiled=True)  80.4 us
    all_gather x1, waiting for transfers between devices, per_device(): lax.all_gather(w_out_fox, 'sp', axis=1, tiled=True)  58.9 us
    all_gather x1, waiting for transfers between devices, per_device(): keys = lax.all_gather(fox_key, 'sp', axis=0, tiled=True)  44.9 us
    all_gather x1, blocking collectives, prefix(): gathered = jax.tree.map(lambda a: lax.all_gather(a, axis), part)  41.5 us
    all_gather x1, blocking collectives, per_device(): gates_all = lax.all_gather(fox_gates, 'sp', axis=0, tiled=True)  36.1 us
    dot_general x6, matrix products, per_device(): jnp.dot(piece, matrix, preferred_element_type=jnp.float32)  19.5 us
    unnamed x17, local copies, waits for them, and re-layouts  14.3 us
  transfers between devices with their start and end apart: 7, of which 6 were waited for; matrix products, arithmetic and copies ran while one was open for 11% of the time, Pallas kernels for 0%

commit v1 on v0

--- a/solution.py
+++ b/solution.py
@@ -238,7 +238,7 @@
     fox_mixed = head_norm(fox_raw, FOX_DIM)
     out_ret, out_fox = (
         lax.all_gather(w_out_ret, "sp", axis=1, tiled=True),
-        lax.all_gather(w_out_fox, "sp", axis=1, tiled=True),
+        jnp.concatenate(lax.all_gather(w_out_fox, "sp"), axis=1),
     )
     return lax.psum_scatter(
         (

time: 544 us -> 543 us (level)
    all_gather x1, waiting for transfers between devices: 58.9 us -> 0.02 us  [per_device(): lax.all_gather(w_out_fox, 'sp')]
    all_gather x1, waiting for transfers between devices: 0.02 us -> 32.3 us  [per_device(): values = lax.all_gather(fox_value, 'sp', axis=0, tiled=True)]
    all_gather x1, waiting for transfers between devices: 44.9 us -> 70.5 us  [per_device(): keys = lax.all_gather(fox_key, 'sp', axis=0, tiled=True)]
    unnamed x17 -> x19, local copies, waits for them, and re-layouts: 14.3 us -> 14.3 us
where the time goes in v1:
time: 543 us; the launch traced here: 541 us
  waiting for transfers between devices  374 us (69%)
  blocking collectives  77.5 us (14%)
  matrix products  32.6 us (6%)
  local copies, waits for them, and re-layouts  31.4 us (6%)
  between operations  13.8 us (3%)
  loops' own time  5.98 us (1%)
    all_gather x1, waiting for transfers between devices, prefix(): gathered = jax.tree.map(lambda a: lax.all_gather(a, axis), part)  172 us
    all_gather x1, waiting for transfers between devices, per_device(): lax.all_gather(w_out_ret, 'sp', axis=1, tiled=True)  80.4 us
    all_gather x1, waiting for transfers between devices, per_device(): keys = lax.all_gather(fox_key, 'sp', axis=0, tiled=True)  70.5 us
    all_gather x1, blocking collectives, prefix(): gathered = jax.tree.map(lambda a: lax.all_gather(a, axis), part)  41.2 us
    all_gather x1, blocking collectives, per_device(): gates_all = lax.all_gather(fox_gates, 'sp', axis=0, tiled=True)  36.3 us
    all_gather x1, waiting for transfers between devices, per_device(): values = lax.all_gather(fox_value, 'sp', axis=0, tiled=True)  32.3 us
    dot_general x6, matrix products, per_device(): jnp.dot(piece, matrix, preferred_element_type=jnp.float32)  19.4 us
    unnamed x19, local copies, waits for them, and re-layouts  14.3 us
  transfers between devices with their start and end apart: 7, of which 6 were waited for; matrix products, arithmetic and copies ran while one was open for 11% of the time, Pallas kernels for 0%

profile of v1, /device:TPU:0, one launch (start us, length us, event | category | flops | bytes accessed | tf_op | source)
XLA Modules:
  0.0 541.1 jit_solution(8017694805485030638)
XLA Ops:
  6.5 1.4 fusion.62
  7.9 2.0 fusion.64
  10.8 11.1 %all-gather.10.cloned.1.call-done = bf16[256,2048]{1,0:T(8,128)(2,1)} async-done(((bf16[128,2048]{1,0:T(8,128)(2,1)}), bf16[256,2048]{1,0:T(8,128)(2,1)}) %all-gather.10.cloned.1.call-update) | async-done | bytes 1048592 | tf_op jit(solution)/shard_map/all_gather | solution.py:169
  21.9 2.7 convolution_convert_fusion.5
  24.7 3.0 convolution_convert_fusion.4
  28.4 3.4 fusion.60
  32.3 3.9 fusion.59
  36.2 1.5 reshape.297
  37.7 3.8 convolution_convert_fusion.1
  41.9 1.4 fusion.71
  43.7 1.4 while.52
  45.1 1.0 copy-done.2
  46.8 41.2 %all-gather.2 = f32[16,1,4]{2,1,0:T(1,128)S(1)} all-gather(f32[1,1,4]{2,1,0:T(1,128)S(1)} %exponential_bitcast_fusion), channel_id=1, replica_groups=mesh['sp'=16,'tp'=2] {'sp'}, dimensions={0}, use_global_device_ids=true | all-gather | bytes 272 | tf_op jit(solution)/shard_map/all_gather | solution.py:16
  88.0 36.3 %all_gather.38 = f32[4096,4]{0,1:T(4,128)S(1)} all-gather(f32[256,4]{0,1:T(4,128)S(1)} %copy-done.5), channel_id=1, replica_groups=mesh['sp'=16,'tp'=2] {'sp'}, dimensions={0}, use_global_device_ids=true | all-gather | bytes 69632 | tf_op jit(solution)/shard_map/all_gather | solution.py:203
  124.4 2.7 fusion.61
  127.2 3.9 copy.103
  131.1 32.3 %all-gather.14.cloned.1.call-done = bf16[4096,512]{1,0:T(8,128)(2,1)} async-done(((bf16[256,512]{1,0:T(8,128)(2,1)}), bf16[4096,512]{1,0:T(8,128)(2,1)}) %all-gather.14.cloned.1.call-update) | async-done | bytes 4194320 | tf_op jit(solution)/shard_map/all_gather | solution.py:209
  163.5 6.4 %copy.100 = bf16[4096,512]{0,1:T(8,128)(2,1)} copy(bf16[4096,512]{1,0:T(8,128)(2,1)} %all-gather.14.cloned.1.call-done) | data formatting | bytes 8388608
  169.9 70.5 %all-gather.16.cloned.1.call-done = bf16[4096,512]{1,0:T(8,128)(2,1)} async-done(((bf16[256,512]{1,0:T(8,128)(2,1)}), bf16[4096,512]{1,0:T(8,128)(2,1)}) %all-gather.16.cloned.1.call-update) | async-done | bytes 4194320 | tf_op jit(solution)/shard_map/all_gather | solution.py:208
  240.3 6.4 %copy.101 = bf16[4096,512]{0,1:T(8,128)(2,1)} copy(bf16[4096,512]{1,0:T(8,128)(2,1)} %all-gather.16.cloned.1.call-done) | data formatting | bytes 8388608
  246.8 13.7 %while.51 = (s32[]{:T(128)}, f32[256,4,128]{0,2,1:T(8,128)S(1)}, f32[256,4]{0,1:T(4,128)S(1)}, s32[8]{0:T(128)S(1)}, s32[]{:T(128)}, /*index=5*/bf16[4096,512]{0...) while((s32[]{:T(128)}, f32[256,4,128]{0,2,1:T(8,128)S(1)}, ...), condition=%wide.region_12.13_spmd.clone, body=%wide.region_8.12_spmd.clone.sunk | while | flops 271844096 | bytes 6869325 | solution.py:233
  248.1 3.4 conditional.3
  248.1 1.9 constant_dynamic-slice_fusion
  260.7 171.9 %all-gather.18.cloned.1.call-done = f32[64,256,256]{2,1,0:T(8,128)} async-done(((f32[4,256,256]{2,1,0:T(8,128)}), f32[64,256,256]{2,1,0:T(8,128)}) %all-gather.18.cloned.1.call-update) | async-done | bytes 16777232 | tf_op jit(solution)/shard_map/all_gather | solution.py:16
  432.9 6.1 %while.53 = (s32[]{:T(128)}, f32[4,256,256]{2,1,0:T(8,128)S(1)}, f32[2,128,4,256]{1,3,2,0:T(8,128)}, bf16[2,128,4,256]{3,1,0,2:T(8,128)(2,1)S(1)}, bf16[2,128,4,...) while((s32[]{:T(128)}, f32[4,256,256]{2,1,0:T(8,128)S(1)}, ...), condition=%wide.region_6.7_spmd.clone.clone, body=%wide.region_5.6_spmd.clone.clone.sunk | while | flops 538313792 | bytes 6387361 | solution.py:108
  433.3 1.9 fusion.110
  436.4 1.8 fusion.110
  438.9 1.7 copy.98
  441.7 80.4 %all-gather.12.cloned.1.call-done = bf16[1024,2048]{1,0:T(8,128)(2,1)} async-done(((bf16[1024,128]{1,0:T(8,128)(2,1)}), bf16[1024,2048]{1,0:T(8,128)(2,1)}) %all-gather.12.cloned.1.call-update) | async-done | bytes 4194320 | tf_op jit(solution)/shard_map/all_gather | solution.py:240
  522.1 3.6 fusion.66
  525.7 1.8 fusion.58
  527.5 6.7 %reduce-scatter.2.cloned.1.call-done = bf16[128,2048]{1,0:T(8,128)(2,1)} async-done(((bf16[256,2048]{1,0:T(8,128)(2,1)}), bf16[128,2048]{1,0:T(8,128)(2,1)}) %reduce-scatter.2.cloned.1.call-update) | async-done | bytes 524304 | tf_op jit(solution)/shard_map/reduce_scatter | solution.py:243
  (108 shorter events, 15.0 us)
Async XLA Ops:
  6.5 15.4 %copy-start = (bf16[2048,512]{1,0:T(8,128)(2,1)S(1)}, bf16[2048,512]{1,0:T(8,128)(2,1)}, u32[]{:S(2)}) copy-start(bf16[2048,512]{1,0:T(8,128)(2,1)} %param.28) | copy-start | bytes 6291460
  6.5 15.3 %all-gather.10.cloned.1.call-start = ((), (), s32[]{:S(2)}) async-start(), calls=%async_computation.1 | async-start | bytes 1572864 | tf_op jit(solution)/shard_map/all_gather | solution.py:169
  10.0 117.2 %all-gather.20.cloned.1.call-start = ((), (), s32[]{:S(2)}) async-start(), calls=%async_computation.7 | async-start | bytes 2228224 | tf_op jit(solution)/shard_map/all_gather | solution.py:241
  10.7 152.7 %all-gather.14.cloned.1.call-start = ((), (), s32[]{:S(2)}) async-start(), calls=%async_computation.3 | async-start | bytes 4456448 | tf_op jit(solution)/shard_map/all_gather | solution.py:209
  21.9 2.8 copy-start.6
  24.6 215.7 %all-gather.16.cloned.1.call-start = ((), (), s32[]{:S(2)}) async-start(), calls=%async_computation.4 | async-start | bytes 4456448 | tf_op jit(solution)/shard_map/all_gather | solution.py:208
  27.7 404.9 %all-gather.18.cloned.1.call-start = ((), (), s32[]{:S(2)}) async-start(), calls=%async_computation.6 | async-start | bytes 17825792 | tf_op jit(solution)/shard_map/all_gather | solution.py:16
  43.7 44.3 %copy-start.5 = (f32[256,4]{0,1:T(4,128)S(1)}, f32[256,4]{0,1:T(4,128)}, u32[]{:S(2)}) copy-start(f32[256,4]{0,1:T(4,128)} %param.29) | copy-start | bytes 12292
  45.1 1.0 copy-start.2
  46.2 475.9 %all-gather.12.cloned.1.call-start = ((), (), s32[]{:S(2)}) async-start(), calls=%async_computation.2 | async-start | bytes 4456448 | tf_op jit(solution)/shard_map/all_gather | solution.py:240
  46.7 487.5 %reduce-scatter.2.cloned.1.call-start = ((), (), s32[]{:S(2)}) async-start(), calls=%async_computation.5 | async-start | bytes 1572864 | tf_op jit(solution)/shard_map/reduce_scatter | solution.py:243
  438.9 1.7 copy-start.4
  522.1 3.6 copy-start.3
  525.7 8.6 %copy-start.1 = (bf16[2048,512]{1,0:T(8,128)(2,1)S(1)}, bf16[2048,512]{1,0:T(8,128)(2,1)}, u32[]{:S(2)}) copy-start(bf16[2048,512]{1,0:T(8,128)(2,1)} %param.28) | copy-start | bytes 6291460
Sparse Core Ops, SparseCore 0:
  10.1 11.7 all-gather.9
  24.7 61.7 all-gather.19
  89.2 74.1 all-gather.13
  166.1 74.1 all-gather.15
  242.9 189.5 all-gather.17
  435.1 86.8 all-gather.11
  527.6 6.5 reduce-scatter.1
